TPU v7x, 32 devices: a whole 2x2x4 slice. The times are simulated.
32 devices in a mesh: sp: 8 (over z, y), tp: 4 (over x, core).
Axes of the slice: x: 2, y: 2, z: 4, core: 2. Of those that a mesh axis runs over, the one named last changes fastest.
Arguments:
- residual_in: bfloat16 [4096, 2048], P('sp'), may hold values from -6 to 6
- queries_nope: bfloat16 [4096, 1024], P('sp', 'tp'), may hold values from -15 to 15
- queries_rope: bfloat16 [4096, 512], P('sp', 'tp'), may hold values from -400 to 400
- latents: bfloat16 [4096, 256], P('sp'), may hold values from -6 to 6
- rope_keys: bfloat16 [4096, 32], P('sp'), may hold values from -8 to 8
- latent_norm_gain: float32 [256], replicated, may hold values from 0.1 to 1.9
- key_up_weight: bfloat16 [256, 1024], P(None, 'tp'), may hold values from -0.375 to 0.375
- value_up_weight: bfloat16 [256, 1024], P(None, 'tp'), may hold values from -0.375 to 0.375
- w_out: bfloat16 [1024, 2048], P('tp'), may hold values from -0.59765625 to 0.59765625
- norm_gain: float32 [2048], replicated, may hold values from 0.1 to 1.9
- w_up: bfloat16 [2048, 8192], P('sp', 'tp'), may hold values from -0.125 to 0.125
- w_down: bfloat16 [8192, 2048], P('tp', 'sp'), may hold values from -0.0625 to 0.0625
Outputs:
- layer_out: bfloat16 [4096, 2048], P('sp', 'tp')
All inputs are finite; a program needn't handle non-finite values.
Results may differ from a plain program's by a relative error of at most 0.015.
Values may be sent and summed in bfloat16 or wider, within the bound.
A program may use at most 128 MiB of HBM per device.

v0:
```python
import math
import jax
import jax.numpy as jnp
from jax import lax
from jax.sharding import PartitionSpec as P

UNROTATED_WIDTH = 64
ROPE = 32
rope_base = 10000.0
epsilon = 1e-06


def rotate(vectors, phases):
    half_width = vectors.shape[-1] // 2
    first_half = vectors[..., :half_width]
    second_half = vectors[..., half_width:]
    cosine = jnp.cos(phases)
    sine = jnp.sin(phases)
    return jnp.concatenate(
        [first_half * cosine - second_half * sine, second_half * cosine + first_half * sine],
        axis=-1,
    )


def rope_phases(positions, width):
    inverse = 1.0 / rope_base ** (jnp.arange(0, width, 2, dtype=jnp.float32) / width)
    return positions.astype(jnp.float32)[:, None] * inverse[None, :]


def rms_scale(vectors, gain_vec):
    return (
        vectors
        * lax.rsqrt(jnp.mean(vectors * vectors, axis=-1, keepdims=True) + epsilon)
        * gain_vec
    )


def attend_block(carry, queries, key_nope, value_rows, key_rot):
    row_peak, denominator, accum = carry
    key_count = key_nope.shape[0]
    heads = queries.shape[1]
    key_all = jnp.concatenate(
        [key_nope, jnp.broadcast_to(key_rot[:, None, :], (key_count, heads, key_rot.shape[1]))],
        axis=2,
    )
    scores = jnp.einsum("qhd,khd->hqk", queries, key_all, preferred_element_type=jnp.float32) * (
        1.0 / math.sqrt(UNROTATED_WIDTH + ROPE)
    )
    new_peak = jnp.maximum(row_peak, jnp.max(scores, axis=2))
    factor = jnp.exp(row_peak - new_peak)
    weights = jnp.exp(scores - new_peak[:, :, None])
    denominator = denominator * factor + jnp.sum(weights, axis=2)
    accum = accum * jnp.transpose(factor)[:, :, None] + jnp.einsum(
        "hqk,khd->qhd", weights.astype(jnp.bfloat16), value_rows, preferred_element_type=jnp.float32
    )
    return (new_peak, denominator, accum)


def fold_blocks(carry, pieces, expand, queries):
    count = pieces[0].shape[0]
    width = math.gcd(count, 1024)

    def one_block(state, start):
        sliced = tuple((lax.dynamic_slice_in_dim(member, start, width, 0) for member in pieces))
        key_nope, value_rows, key_rot = expand(sliced)
        return attend_block(state, queries, key_nope, value_rows, key_rot)

    return lax.fori_loop(
        0, count // width, lambda turn, state: one_block(state, turn * width), carry
    )


def on_device(
    residual_in,
    queries_nope,
    queries_rope,
    latents,
    rope_keys,
    latent_norm_gain,
    key_up_weight,
    value_up_weight,
    w_out,
    norm_gain,
    w_up,
    w_down,
):
    rows = residual_in.shape[0]
    heads = key_up_weight.shape[1] // UNROTATED_WIDTH
    value_width = value_up_weight.shape[1] // heads
    positions = lax.axis_index("sp") * rows + jnp.arange(rows, dtype=jnp.int32)
    phases = rope_phases(positions, ROPE)
    q_rot = rotate(
        queries_rope.astype(jnp.float32).reshape(rows, heads, ROPE), phases[:, None, :]
    ).astype(jnp.bfloat16)
    queries = jnp.concatenate([queries_nope.reshape(rows, heads, UNROTATED_WIDTH), q_rot], axis=2)
    lat_norm = rms_scale(latents.astype(jnp.float32), latent_norm_gain).astype(jnp.bfloat16)
    key_rot = rotate(rope_keys.astype(jnp.float32), phases).astype(jnp.bfloat16)
    start_carry = (
        jnp.full((heads, rows), -1e30, jnp.float32),
        jnp.zeros((heads, rows), jnp.float32),
        jnp.zeros((rows, heads, value_width), jnp.float32),
    )

    def expand_latent(sliced):
        lat_rows, rot_rows = sliced
        count = lat_rows.shape[0]
        key_nope = (
            jnp.dot(lat_rows, key_up_weight, preferred_element_type=jnp.float32)
            .astype(jnp.bfloat16)
            .reshape(count, heads, UNROTATED_WIDTH)
        )
        value_rows = (
            jnp.dot(lat_rows, value_up_weight, preferred_element_type=jnp.float32)
            .astype(jnp.bfloat16)
            .reshape(count, heads, value_width)
        )
        return (key_nope, value_rows, rot_rows)

    result = fold_blocks(
        start_carry,
        (
            lax.all_gather(lat_norm, "sp", axis=0, tiled=True),
            lax.all_gather(key_rot, "sp", axis=0, tiled=True),
        ),
        expand_latent,
        queries,
    )
    row_peak, denominator, accum = result
    attended = (
        (accum / jnp.transpose(denominator)[:, :, None])
        .astype(jnp.bfloat16)
        .reshape(rows, heads * value_width)
    )
    part_term = jnp.dot(attended, w_out, preferred_element_type=jnp.float32)
    summed = lax.psum(part_term.astype(jnp.bfloat16), "tp").astype(jnp.float32)
    stream = residual_in.astype(jnp.float32) + summed
    normed = rms_scale(stream, norm_gain).astype(jnp.bfloat16)
    upward = jnp.dot(
        normed, lax.all_gather(w_up, "sp", axis=0, tiled=True), preferred_element_type=jnp.float32
    )
    hidden = jnp.square(jax.nn.relu(upward)).astype(jnp.bfloat16)
    terms = jnp.dot(
        hidden, lax.all_gather(w_down, "sp", axis=1, tiled=True), preferred_element_type=jnp.float32
    )
    mixer = lax.psum_scatter(
        terms.astype(jnp.bfloat16), "tp", scatter_dimension=1, tiled=True
    ).astype(jnp.float32)
    own_width = mixer.shape[1]
    own_stream = lax.dynamic_slice_in_dim(stream, lax.axis_index("tp") * own_width, own_width, 1)
    return (own_stream + mixer).astype(jnp.bfloat16)


def solution(mesh):
    in_specs = (
        P("sp", None),
        P("sp", "tp"),
        P("sp", "tp"),
        P("sp", None),
        P("sp", None),
        P(),
        P(None, "tp"),
        P(None, "tp"),
        P("tp", None),
        P(),
        P("sp", "tp"),
        P("tp", "sp"),
    )
    out_specs = P("sp", "tp")
    return jax.shard_map(
        on_device, mesh=mesh, in_specs=in_specs, out_specs=out_specs, check_vma=False
    )
```

profile of v0, /device:TPU:0, one launch (start us, length us, event | category | flops | bytes accessed | tf_op | source)
XLA Modules:
  0.0 480.2 jit_solution(10684508900544184789)
XLA Ops:
  7.7 1.8 fusion.27
  12.8 33.2 %all_gather.13 = bf16[4096,32]{0,1:T(8,128)(2,1)S(1)} all-gather(bf16[512,32]{0,1:T(8,128)(2,1)S(1)} %pad_maximum_fusion.1), channel_id=1, replica_groups=mesh['sp'=8,'tp'=4] {'sp'}, dimensions={0}, use_global_device_ids=true | all-gather | bytes 294912 | tf_op jit(solution)/shard_map/all_gather | solution.py:123
  46.0 16.1 %all-gather.4.cloned.1.call-done = bf16[4096,256]{1,0:T(8,128)(2,1)} async-done(((bf16[512,256]{1,0:T(8,128)(2,1)}), bf16[4096,256]{1,0:T(8,128)(2,1)}) %all-gather.4.cloned.1.call-update) | async-done | bytes 2097168 | tf_op jit(solution)/shard_map/all_gather | solution.py:122
  62.1 58.6 %while.18 = (s32[]{:T(128)}, f32[4,512]{1,0:T(4,128)S(1)}, f32[4,512]{1,0:T(4,128)S(1)}, f32[512,4,64]{0,2,1:T(8,128)S(1)}, bf16[4096,256]{1,0:T(8,128)(2,1)}, /...) while((s32[]{:T(128)}, f32[4,512]{1,0:T(4,128)S(1)}, ...), condition=%wide.region_4.0_spmd.clone, body=%wide.region_1.0_spmd.clone.sunk | while | flops 958803968 | bytes 64946424 | solution.py:68
  62.1 1.4 convolution_convert_fusion.6
  63.6 4.5 bitcast_reduce_fusion.2
  68.2 1.4 convolution_convert_fusion.7
  69.6 5.1 %fusion.62 = f32[512,4,64]{0,2,1:T(8,128)S(1)} fusion(bf16[1024,4,64]{0,2,1:T(8,128)(2,1)S(1)} %bitcast.61, f32[4,1024,512]{2,1,0:T(8,128)} %get-tuple-element.285, f32[4,512]{1,0:T(4,128)S(1)} %get-tuple-element.314, f32[512,4,64]{0,2,1:T(8,128)S(1)} %get-tuple-element.303, f32[512,4]{0,1:T(4,128)S(1)} %get-tuple-element.286, pred[]{:T(512)S(6)} %compare.3), kind=kOutput, calls=%fused_computation.9.clone.1 | convolution fusion | flops 275120128 | bytes 9977857 | tf_op jit(solution)/shard_map/while/body/eval_jaxpr/hqk,khd->qhd/dot_general | solution.py:53
  75.3 1.4 fusion.60
  76.8 1.4 convolution_convert_fusion.6
  78.3 4.5 bitcast_reduce_fusion.2
  82.8 1.4 convolution_convert_fusion.7
  84.2 5.1 %fusion.62 = f32[512,4,64]{0,2,1:T(8,128)S(1)} fusion(bf16[1024,4,64]{0,2,1:T(8,128)(2,1)S(1)} %bitcast.61, f32[4,1024,512]{2,1,0:T(8,128)} %get-tuple-element.285, f32[4,512]{1,0:T(4,128)S(1)} %get-tuple-element.314, f32[512,4,64]{0,2,1:T(8,128)S(1)} %get-tuple-element.303, f32[512,4]{0,1:T(4,128)S(1)} %get-tuple-element.286, pred[]{:T(512)S(6)} %compare.3), kind=kOutput, calls=%fused_computation.9.clone.1 | convolution fusion | flops 275120128 | bytes 9977857 | tf_op jit(solution)/shard_map/while/body/eval_jaxpr/hqk,khd->qhd/dot_general | solution.py:53
  90.0 1.4 fusion.60
  91.4 1.4 convolution_convert_fusion.6
  92.9 4.5 bitcast_reduce_fusion.2
  97.5 1.4 convolution_convert_fusion.7
  98.9 5.1 %fusion.62 = f32[512,4,64]{0,2,1:T(8,128)S(1)} fusion(bf16[1024,4,64]{0,2,1:T(8,128)(2,1)S(1)} %bitcast.61, f32[4,1024,512]{2,1,0:T(8,128)} %get-tuple-element.285, f32[4,512]{1,0:T(4,128)S(1)} %get-tuple-element.314, f32[512,4,64]{0,2,1:T(8,128)S(1)} %get-tuple-element.303, f32[512,4]{0,1:T(4,128)S(1)} %get-tuple-element.286, pred[]{:T(512)S(6)} %compare.3), kind=kOutput, calls=%fused_computation.9.clone.1 | convolution fusion | flops 275120128 | bytes 9977857 | tf_op jit(solution)/shard_map/while/body/eval_jaxpr/hqk,khd->qhd/dot_general | solution.py:53
  104.6 1.4 fusion.60
  106.1 1.4 convolution_convert_fusion.6
  107.6 4.5 bitcast_reduce_fusion.2
  112.1 1.4 convolution_convert_fusion.7
  113.5 5.1 %fusion.62 = f32[512,4,64]{0,2,1:T(8,128)S(1)} fusion(bf16[1024,4,64]{0,2,1:T(8,128)(2,1)S(1)} %bitcast.61, f32[4,1024,512]{2,1,0:T(8,128)} %get-tuple-element.285, f32[4,512]{1,0:T(4,128)S(1)} %get-tuple-element.314, f32[512,4,64]{0,2,1:T(8,128)S(1)} %get-tuple-element.303, f32[512,4]{0,1:T(4,128)S(1)} %get-tuple-element.286, pred[]{:T(512)S(6)} %compare.3), kind=kOutput, calls=%fused_computation.9.clone.1 | convolution fusion | flops 275120128 | bytes 9977857 | tf_op jit(solution)/shard_map/while/body/eval_jaxpr/hqk,khd->qhd/dot_general | solution.py:53
  119.3 1.4 fusion.60
  120.8 2.1 convolution_convert_fusion.2
  124.5 48.9 %all-reduce.2.cloned.1.call-done = bf16[512,2048]{1,0:T(8,128)(2,1)} async-done(((bf16[512,2048]{1,0:T(8,128)(2,1)}), bf16[512,2048]{1,0:T(8,128)(2,1)}) %all-reduce.2.cloned.1.call-update) | async-done | bytes 2097168 | tf_op jit(solution)/shard_map/psum | solution.py:135
  173.4 4.2 convert_add_fusion
  177.6 122.5 %all-gather.6.cloned.1.call-done = bf16[2048,2048]{1,0:T(8,128)(2,1)} async-done(((bf16[256,2048]{1,0:T(8,128)(2,1)}), bf16[2048,2048]{1,0:T(8,128)(2,1)}) %all-gather.6.cloned.1.call-update) | async-done | bytes 8388624 | tf_op jit(solution)/shard_map/all_gather | solution.py:139
  300.1 125.0 %all-gather.8.cloned.1.call-done = bf16[2048,2048]{1,0:T(8,128)(2,1)} async-done(((bf16[2048,256]{1,0:T(8,128)(2,1)}), bf16[2048,2048]{1,0:T(8,128)(2,1)}) %all-gather.8.cloned.1.call-update) | async-done | bytes 8388624 | tf_op jit(solution)/shard_map/all_gather | solution.py:143
  425.2 16.6 %convolution_convert_fusion.3 = bf16[512,2048]{1,0:T(8,128)(2,1)} fusion(bf16[2048,2048]{1,0:T(8,128)(2,1)} %all-gather.8.cloned.1.call-done, bf16[2048,2048]{1,0:T(8,128)(2,1)} %all-gather.6.cloned.1.call-done, f32[2048]{0:T(1024)S(1)} %copy-done.4, f32[512]{0:T(512)S(1)} %add_rsqrt_fusion, bf16[512,2048]{1,0:T(8,128)(2,1)} %all-reduce.2.cloned.1.call-done, ...), kind=kOutput, calls=%fused_computation.32 | convolution fusion | flops 8600420352 | bytes 23078912 | tf_op jit(solution)/shard_map/dot_general | solution.py:142
  441.8 29.5 %reduce-scatter.2.cloned.1.call-done = bf16[512,512]{1,0:T(8,128)(2,1)} async-done(((bf16[512,2048]{1,0:T(8,128)(2,1)}), bf16[512,512]{1,0:T(8,128)(2,1)}) %reduce-scatter.2.cloned.1.call-update) | async-done | bytes 524304 | tf_op jit(solution)/shard_map/reduce_scatter | solution.py:145
  471.3 2.3 add_convert_fusion
  (68 shorter events, 8.7 us)
Async XLA Ops:
  6.5 114.3 %copy-start = (bf16[256,2048]{1,0:T(8,128)(2,1)S(1)}, bf16[256,2048]{1,0:T(8,128)(2,1)}, u32[]{:S(2)}) copy-start(bf16[256,2048]{1,0:T(8,128)(2,1)} %param.22) | copy-start | bytes 3145732
  6.5 55.6 %all-gather.4.cloned.1.call-start = ((), (), s32[]{:S(2)}) async-start(), calls=%async_computation.1 | async-start | bytes 2359296 | tf_op jit(solution)/shard_map/all_gather | solution.py:122
  9.6 163.9 %all-reduce.2.cloned.1.call-start = ((), (), s32[]{:S(2)}) async-start(), calls=%async_computation.2 | async-start | bytes 4194304 | tf_op jit(solution)/shard_map/psum | solution.py:135
  63.6 4.6 copy-start.2
  69.6 5.8 %copy-start.1 = (f32[4,1024,512]{2,1,0:T(8,128)S(1)}, f32[4,1024,512]{2,1,0:T(8,128)}, u32[]{:S(2)}) copy-start(f32[4,1024,512]{2,1,0:T(8,128)} %get-tuple-element.285) | copy-start | bytes 25165828 | tf_op jit(solution)/shard_map/while
  78.2 4.6 copy-start.2
  84.2 5.8 %copy-start.1 = (f32[4,1024,512]{2,1,0:T(8,128)S(1)}, f32[4,1024,512]{2,1,0:T(8,128)}, u32[]{:S(2)}) copy-start(f32[4,1024,512]{2,1,0:T(8,128)} %get-tuple-element.285) | copy-start | bytes 25165828 | tf_op jit(solution)/shard_map/while
  92.9 4.6 copy-start.2
  98.9 5.8 %copy-start.1 = (f32[4,1024,512]{2,1,0:T(8,128)S(1)}, f32[4,1024,512]{2,1,0:T(8,128)}, u32[]{:S(2)}) copy-start(f32[4,1024,512]{2,1,0:T(8,128)} %get-tuple-element.285) | copy-start | bytes 25165828 | tf_op jit(solution)/shard_map/while
  107.5 4.6 copy-start.2
  113.5 5.8 %copy-start.1 = (f32[4,1024,512]{2,1,0:T(8,128)S(1)}, f32[4,1024,512]{2,1,0:T(8,128)}, u32[]{:S(2)}) copy-start(f32[4,1024,512]{2,1,0:T(8,128)} %get-tuple-element.285) | copy-start | bytes 25165828 | tf_op jit(solution)/shard_map/while
  120.8 52.6 %copy-start.3 = (bf16[512,2048]{1,0:T(8,128)(2,1)S(1)}, bf16[512,2048]{1,0:T(8,128)(2,1)}, u32[]{:S(2)}) copy-start(bf16[512,2048]{1,0:T(8,128)(2,1)} %param.14) | copy-start | bytes 6291460
  122.9 177.2 %all-gather.6.cloned.1.call-start = ((), (), s32[]{:S(2)}) async-start(), calls=%async_computation.3 | async-start | bytes 9437184 | tf_op jit(solution)/shard_map/all_gather | solution.py:139
  123.7 301.5 %all-gather.8.cloned.1.call-start = ((), (), s32[]{:S(2)}) async-start(), calls=%async_computation.4 | async-start | bytes 9437184 | tf_op jit(solution)/shard_map/all_gather | solution.py:143
  124.2 300.9 %copy-start.4 = (f32[2048]{0:T(1024)S(1)}, f32[2048]{0:T(1024)}, u32[]{:S(2)}) copy-start(f32[2048]{0:T(1024)} %param.23) | copy-start | bytes 24580
  124.3 347.1 %reduce-scatter.2.cloned.1.call-start = ((), (), s32[]{:S(2)}) async-start(), calls=%async_computation.5 | async-start | bytes 2621440 | tf_op jit(solution)/shard_map/reduce_scatter | solution.py:145
Sparse Core Ops, SparseCore 0:
  9.7 52.4 all-gather.3
  123.0 50.3 all-reduce.1
  175.6 124.5 all-gather.5
  302.0 123.1 all-gather.7
  441.9 29.3 reduce-scatter.1
where the time goes:
time: 481 us; the launch traced here: 480 us
  waiting for transfers between devices  343 us (71%)
  matrix products  68.6 us (14%)
  blocking collectives  33.2 us (7%)
  other arithmetic  16.3 us (3%)
  between operations  13.3 us (3%)
    all_gather x1, waiting for transfers between devices, on_device(): lax.all_gather(w_down, 'sp', axis=1, tiled=True)  125 us
    all_gather x1, waiting for transfers between devices, on_device(): lax.all_gather(w_up, 'sp', axis=0, tiled=True)  123 us
    psum x1, waiting for transfers between devices, on_device(): summed = lax.psum(part_term.astype(jnp.bfloat16), 'tp').astype(jnp.float32)  48.9 us
    all_gather x1, blocking collectives, on_device(): lax.all_gather(key_rot, 'sp', axis=0, tiled=True)  33.2 us
    reduce_scatter x1, waiting for transfers between devices, on_device(): lax.psum_scatter(terms.astype(jnp.bfloat16), 'tp', scatter_dimension=1, t...  29.5 us
    dot_general x4, matrix products, attend_block(): jnp.einsum('hqk,khd->qhd', weights.astype(jnp.bfloat16), value_rows, pref...  20.6 us
    dot_general x4, matrix products, attend_block(): jnp.einsum('qhd,khd->hqk', queries, key_all, preferred_element_type=jnp.f...  18.2 us
    dot_general x1, matrix products, on_device(): jnp.dot(hidden, lax.all_gather(w_down, 'sp', axis=1, tiled=True), preferr...  16.6 us
  transfers between devices with their start and end apart: 5, of which 5 were waited for; matrix products, arithmetic and copies ran while one was open for 2% of the time, Pallas kernels for 0%

commit v1 on v0

--- a/solution.py
+++ b/solution.py
@@ -120,7 +120,9 @@
         start_carry,
         (
             lax.all_gather(lat_norm, "sp", axis=0, tiled=True),
-            lax.all_gather(key_rot, "sp", axis=0, tiled=True),
+            jnp.concatenate(
+                lax.all_to_all(jnp.stack([key_rot] * lax.axis_size("sp")), "sp", 0, 0), axis=0
+            ),
         ),
         expand_latent,
         queries,

time: 481 us -> 483 us (level)
  blocking collectives: 33.2 us -> 0 us
  waiting for transfers between devices: 343 us -> 370 us
  starting transfers between devices: 0.34 us -> 7.65 us
    all_gather x1 -> x0, blocking collectives: 33.2 us -> none  [on_device(): lax.all_gather(key_rot, 'sp', axis=0, tiled=True)]
    all_gather x1, waiting for transfers between devices: 16.1 us -> 31.7 us  [on_device(): lax.all_gather(lat_norm, 'sp', axis=0, tiled=True)]
    all_to_all x0 -> x1, waiting for transfers between devices: none -> 11.7 us  [on_device(): lax.all_to_all(jnp.stack([key_rot] * lax.axis_size('sp')), 'sp', 0, 0)]
    all_to_all x0 -> x1, starting transfers between devices: none -> 7.31 us  [on_device(): lax.all_to_all(jnp.stack([key_rot] * lax.axis_size('sp')), 'sp', 0, 0)]
  transfers between devices with their start and end apart: 5 -> 6, of which waited for: 5 -> 6; matrix products, arithmetic and copies ran while one was open for 2% -> 2% of each run, Pallas kernels for 0% -> 0%
where the time goes in v1:
time: 483 us; the launch traced here: 482 us
  waiting for transfers between devices  370 us (77%)
  matrix products  68.5 us (14%)
  other arithmetic  16.3 us (3%)
  between operations  13.3 us (3%)
  starting transfers between devices  7.65 us (2%)
  local copies, waits for them, and re-layouts  5.46 us (1%)
    all_gather x1, waiting for transfers between devices, on_device(): lax.all_gather(w_down, 'sp', axis=1, tiled=True)  125 us
    all_gather x1, waiting for transfers between devices, on_device(): lax.all_gather(w_up, 'sp', axis=0, tiled=True)  123 us
    psum x1, waiting for transfers between devices, on_device(): summed = lax.psum(part_term.astype(jnp.bfloat16), 'tp').astype(jnp.float32)  48.5 us
    all_gather x1, waiting for transfers between devices, on_device(): lax.all_gather(lat_norm, 'sp', axis=0, tiled=True)  31.7 us
    reduce_scatter x1, waiting for transfers between devices, on_device(): lax.psum_scatter(terms.astype(jnp.bfloat16), 'tp', scatter_dimension=1, t...  29.5 us
    dot_general x4, matrix products, attend_block(): jnp.einsum('hqk,khd->qhd', weights.astype(jnp.bfloat16), value_rows, pref...  20.6 us
    dot_general x4, matrix products, attend_block(): jnp.einsum('qhd,khd->hqk', queries, key_all, preferred_element_type=jnp.f...  18.1 us
    dot_general x1, matrix products, on_device(): jnp.dot(hidden, lax.all_gather(w_down, 'sp', axis=1, tiled=True), preferr...  16.6 us
  transfers between devices with their start and end apart: 6, of which 6 were waited for; matrix products, arithmetic and copies ran while one was open for 2% of the time, Pallas kernels for 0%

profile of v1, /device:TPU:0, one launch (start us, length us, event | category | flops | bytes accessed | tf_op | source)
XLA Modules:
  0.0 481.8 jit_solution(5439868228983769763)
XLA Ops:
  7.8 1.8 fusion.27
  11.3 7.3 %all-to-all-start = ((bf16[8,512,32]{1,2,0:T(8,128)(2,1)}), bf16[8,512,32]{1,2,0:T(8,128)(2,1)S(1)}, u32[]{:S(2)}, u32[]{:S(2)}) async-start(bf16[8,512,32]{1,2,0:T(8,128)(2,1)} %stack.2), calls=%async_computation | async-start | bytes 524288 | tf_op jit(solution)/shard_map/all_to_all | solution.py:124
  20.9 11.7 %all-to-all-done = bf16[8,512,32]{1,2,0:T(8,128)(2,1)S(1)} async-done(((bf16[8,512,32]{1,2,0:T(8,128)(2,1)}), bf16[8,512,32]{1,2,0:T(8,128)(2,1)S(1)}, u32[]{:S(2)}, u32[]{:S(2)}) %all-to-all-start) | async-done | bytes 262176 | tf_op jit(solution)/shard_map/all_to_all | solution.py:124
  32.6 31.7 %all-gather.4.cloned.1.call-done = bf16[4096,256]{1,0:T(8,128)(2,1)} async-done(((bf16[512,256]{1,0:T(8,128)(2,1)}), bf16[4096,256]{1,0:T(8,128)(2,1)}) %all-gather.4.cloned.1.call-update) | async-done | bytes 2097168 | tf_op jit(solution)/shard_map/all_gather | solution.py:122
  64.4 58.4 %while.18 = (s32[]{:T(128)}, f32[4,512]{1,0:T(4,128)S(1)}, f32[4,512]{1,0:T(4,128)S(1)}, f32[512,4,64]{0,2,1:T(8,128)S(1)}, bf16[4096,256]{1,0:T(8,128)(2,1)}, /...) while((s32[]{:T(128)}, f32[4,512]{1,0:T(4,128)S(1)}, ...), condition=%wide.region_4.0_spmd.clone, body=%wide.region_1.0_spmd.clone.sunk | while | flops 958803968 | bytes 64422108 | solution.py:68
  65.8 4.5 bitcast_reduce_fusion.2
  70.4 1.4 convolution_convert_fusion.7
  71.8 5.1 %fusion.62 = f32[512,4,64]{0,2,1:T(8,128)S(1)} fusion(bf16[1024,4,64]{0,2,1:T(8,128)(2,1)S(1)} %bitcast.63, f32[4,1024,512]{2,1,0:T(8,128)} %get-tuple-element.285, f32[4,512]{1,0:T(4,128)S(1)} %get-tuple-element.314, f32[512,4,64]{0,2,1:T(8,128)S(1)} %get-tuple-element.303, f32[512,4]{0,1:T(4,128)S(1)} %get-tuple-element.286, pred[]{:T(512)S(6)} %compare.3), kind=kOutput, calls=%fused_computation.9.clone.1 | convolution fusion | flops 275120128 | bytes 9977857 | tf_op jit(solution)/shard_map/while/body/eval_jaxpr/hqk,khd->qhd/dot_general | solution.py:53
  77.5 1.4 fusion.60
  79.0 1.4 convolution_convert_fusion.6
  80.4 4.5 bitcast_reduce_fusion.2
  84.9 1.4 convolution_convert_fusion.7
  86.4 5.1 %fusion.62 = f32[512,4,64]{0,2,1:T(8,128)S(1)} fusion(bf16[1024,4,64]{0,2,1:T(8,128)(2,1)S(1)} %bitcast.63, f32[4,1024,512]{2,1,0:T(8,128)} %get-tuple-element.285, f32[4,512]{1,0:T(4,128)S(1)} %get-tuple-element.314, f32[512,4,64]{0,2,1:T(8,128)S(1)} %get-tuple-element.303, f32[512,4]{0,1:T(4,128)S(1)} %get-tuple-element.286, pred[]{:T(512)S(6)} %compare.3), kind=kOutput, calls=%fused_computation.9.clone.1 | convolution fusion | flops 275120128 | bytes 9977857 | tf_op jit(solution)/shard_map/while/body/eval_jaxpr/hqk,khd->qhd/dot_general | solution.py:53
  92.1 1.4 fusion.60
  93.6 1.4 convolution_convert_fusion.6
  95.0 4.5 bitcast_reduce_fusion.2
  99.5 1.4 convolution_convert_fusion.7
  100.9 5.1 %fusion.62 = f32[512,4,64]{0,2,1:T(8,128)S(1)} fusion(bf16[1024,4,64]{0,2,1:T(8,128)(2,1)S(1)} %bitcast.63, f32[4,1024,512]{2,1,0:T(8,128)} %get-tuple-element.285, f32[4,512]{1,0:T(4,128)S(1)} %get-tuple-element.314, f32[512,4,64]{0,2,1:T(8,128)S(1)} %get-tuple-element.303, f32[512,4]{0,1:T(4,128)S(1)} %get-tuple-element.286, pred[]{:T(512)S(6)} %compare.3), kind=kOutput, calls=%fused_computation.9.clone.1 | convolution fusion | flops 275120128 | bytes 9977857 | tf_op jit(solution)/shard_map/while/body/eval_jaxpr/hqk,khd->qhd/dot_general | solution.py:53
  106.7 1.4 fusion.60
  108.1 1.4 convolution_convert_fusion.6
  109.6 4.5 bitcast_reduce_fusion.2
  114.1 1.4 convolution_convert_fusion.7
  115.5 5.1 %fusion.62 = f32[512,4,64]{0,2,1:T(8,128)S(1)} fusion(bf16[1024,4,64]{0,2,1:T(8,128)(2,1)S(1)} %bitcast.63, f32[4,1024,512]{2,1,0:T(8,128)} %get-tuple-element.285, f32[4,512]{1,0:T(4,128)S(1)} %get-tuple-element.314, f32[512,4,64]{0,2,1:T(8,128)S(1)} %get-tuple-element.303, f32[512,4]{0,1:T(4,128)S(1)} %get-tuple-element.286, pred[]{:T(512)S(6)} %compare.3), kind=kOutput, calls=%fused_computation.9.clone.1 | convolution fusion | flops 275120128 | bytes 9977857 | tf_op jit(solution)/shard_map/while/body/eval_jaxpr/hqk,khd->qhd/dot_general | solution.py:53
  121.3 1.4 fusion.60
  122.8 2.1 convolution_convert_fusion.2
  126.5 48.5 %all-reduce.2.cloned.1.call-done = bf16[512,2048]{1,0:T(8,128)(2,1)} async-done(((bf16[512,2048]{1,0:T(8,128)(2,1)}), bf16[512,2048]{1,0:T(8,128)(2,1)}) %all-reduce.2.cloned.1.call-update) | async-done | bytes 2097168 | tf_op jit(solution)/shard_map/psum | solution.py:137
  175.0 4.2 convert_add_fusion
  179.2 122.5 %all-gather.6.cloned.1.call-done = bf16[2048,2048]{1,0:T(8,128)(2,1)} async-done(((bf16[256,2048]{1,0:T(8,128)(2,1)}), bf16[2048,2048]{1,0:T(8,128)(2,1)}) %all-gather.6.cloned.1.call-update) | async-done | bytes 8388624 | tf_op jit(solution)/shard_map/all_gather | solution.py:141
  301.7 125.0 %all-gather.8.cloned.1.call-done = bf16[2048,2048]{1,0:T(8,128)(2,1)} async-done(((bf16[2048,256]{1,0:T(8,128)(2,1)}), bf16[2048,2048]{1,0:T(8,128)(2,1)}) %all-gather.8.cloned.1.call-update) | async-done | bytes 8388624 | tf_op jit(solution)/shard_map/all_gather | solution.py:145
  426.8 16.6 %convolution_convert_fusion.3 = bf16[512,2048]{1,0:T(8,128)(2,1)} fusion(bf16[2048,2048]{1,0:T(8,128)(2,1)} %all-gather.8.cloned.1.call-done, bf16[2048,2048]{1,0:T(8,128)(2,1)} %all-gather.6.cloned.1.call-done, f32[2048]{0:T(1024)S(1)} %copy-done.5, f32[512]{0:T(512)S(1)} %add_rsqrt_fusion, bf16[512,2048]{1,0:T(8,128)(2,1)} %all-reduce.2.cloned.1.call-done, ...), kind=kOutput, calls=%fused_computation.32 | convolution fusion | flops 8600420352 | bytes 23078912 | tf_op jit(solution)/shard_map/dot_general | solution.py:144
  443.4 29.5 %reduce-scatter.2.cloned.1.call-done = bf16[512,512]{1,0:T(8,128)(2,1)} async-done(((bf16[512,2048]{1,0:T(8,128)(2,1)}), bf16[512,512]{1,0:T(8,128)(2,1)}) %reduce-scatter.2.cloned.1.call-update) | async-done | bytes 524304 | tf_op jit(solution)/shard_map/reduce_scatter | solution.py:147
  472.9 2.3 add_convert_fusion
  (67 shorter events, 10.9 us)
Async XLA Ops:
  6.5 116.3 %copy-start = (bf16[256,2048]{1,0:T(8,128)(2,1)S(1)}, bf16[256,2048]{1,0:T(8,128)(2,1)}, u32[]{:S(2)}) copy-start(bf16[256,2048]{1,0:T(8,128)(2,1)} %param.22) | copy-start | bytes 3145732
  6.5 57.8 %copy-start.2 = (bf16[256,256]{1,0:T(8,128)(2,1)S(1)}, bf16[256,256]{1,0:T(8,128)(2,1)}, u32[]{:S(2)}) copy-start(bf16[256,256]{1,0:T(8,128)(2,1)} %param.20) | copy-start | bytes 393220
  6.5 57.8 %copy-start.3 = (bf16[256,256]{1,0:T(8,128)(2,1)S(1)}, bf16[256,256]{1,0:T(8,128)(2,1)}, u32[]{:S(2)}) copy-start(bf16[256,256]{1,0:T(8,128)(2,1)} %param.21) | copy-start | bytes 393220
  6.5 57.8 %all-gather.4.cloned.1.call-start = ((), (), s32[]{:S(2)}) async-start(), calls=%async_computation.2 | async-start | bytes 2359296 | tf_op jit(solution)/shard_map/all_gather | solution.py:122
  11.3 21.3 %all-to-all-start = ((bf16[8,512,32]{1,2,0:T(8,128)(2,1)}), bf16[8,512,32]{1,2,0:T(8,128)(2,1)S(1)}, u32[]{:S(2)}, u32[]{:S(2)}) async-start(bf16[8,512,32]{1,2,0:T(8,128)(2,1)} %stack.2), calls=%async_computation | async-start | bytes 524288 | tf_op jit(solution)/shard_map/all_to_all | solution.py:124
  18.6 156.4 %all-reduce.2.cloned.1.call-start = ((), (), s32[]{:S(2)}) async-start(), calls=%async_computation.3 | async-start | bytes 4194304 | tf_op jit(solution)/shard_map/psum | solution.py:137
  71.8 5.8 %copy-start.1 = (f32[4,1024,512]{2,1,0:T(8,128)S(1)}, f32[4,1024,512]{2,1,0:T(8,128)}, u32[]{:S(2)}) copy-start(f32[4,1024,512]{2,1,0:T(8,128)} %get-tuple-element.285) | copy-start | bytes 25165828 | tf_op jit(solution)/shard_map/while
  86.3 5.8 %copy-start.1 = (f32[4,1024,512]{2,1,0:T(8,128)S(1)}, f32[4,1024,512]{2,1,0:T(8,128)}, u32[]{:S(2)}) copy-start(f32[4,1024,512]{2,1,0:T(8,128)} %get-tuple-element.285) | copy-start | bytes 25165828 | tf_op jit(solution)/shard_map/while
  100.9 5.8 %copy-start.1 = (f32[4,1024,512]{2,1,0:T(8,128)S(1)}, f32[4,1024,512]{2,1,0:T(8,128)}, u32[]{:S(2)}) copy-start(f32[4,1024,512]{2,1,0:T(8,128)} %get-tuple-element.285) | copy-start | bytes 25165828 | tf_op jit(solution)/shard_map/while
  115.5 5.8 %copy-start.1 = (f32[4,1024,512]{2,1,0:T(8,128)S(1)}, f32[4,1024,512]{2,1,0:T(8,128)}, u32[]{:S(2)}) copy-start(f32[4,1024,512]{2,1,0:T(8,128)} %get-tuple-element.285) | copy-start | bytes 25165828 | tf_op jit(solution)/shard_map/while
  122.8 52.2 %copy-start.4 = (bf16[512,2048]{1,0:T(8,128)(2,1)S(1)}, bf16[512,2048]{1,0:T(8,128)(2,1)}, u32[]{:S(2)}) copy-start(bf16[512,2048]{1,0:T(8,128)(2,1)} %param.14) | copy-start | bytes 6291460
  124.9 176.8 %all-gather.6.cloned.1.call-start = ((), (), s32[]{:S(2)}) async-start(), calls=%async_computation.4 | async-start | bytes 9437184 | tf_op jit(solution)/shard_map/all_gather | solution.py:141
  125.7 301.1 %all-gather.8.cloned.1.call-start = ((), (), s32[]{:S(2)}) async-start(), calls=%async_computation.5 | async-start | bytes 9437184 | tf_op jit(solution)/shard_map/all_gather | solution.py:145
  126.2 300.5 %copy-start.5 = (f32[2048]{0:T(1024)S(1)}, f32[2048]{0:T(1024)}, u32[]{:S(2)}) copy-start(f32[2048]{0:T(1024)} %param.23) | copy-start | bytes 24580
  126.2 346.6 %reduce-scatter.2.cloned.1.call-start = ((), (), s32[]{:S(2)}) async-start(), calls=%async_computation.6 | async-start | bytes 2621440 | tf_op jit(solution)/shard_map/reduce_scatter | solution.py:147
Sparse Core Ops, SparseCore 0:
  9.7 54.6 all-gather.3
  125.0 49.9 all-reduce.1
  177.1 124.5 all-gather.5
  303.6 123.1 all-gather.7
  443.5 29.3 reduce-scatter.1
